TPU v7x, 32 devices: a whole 2x2x4 slice. The times are simulated.
32 devices in a mesh: sp: 8 (over z, x), tp: 4 (over y, core).
Axes of the slice: x: 2, y: 2, z: 4, core: 2. Of those that a mesh axis runs over, the one named last changes fastest.
Arguments:
- tokens: bfloat16 [4096, 2048], P(('sp', 'tp')), may hold values from -6 to 6
- elapsed: float32 [4096], P(('sp', 'tp')), may hold values from 0 to 3, as said below
- norm_gain: float32 [2048], replicated, may hold values from 0.1 to 1.9
- in_weight: bfloat16 [2048, 1024], replicated, may hold values from -0.125 to 0.125
- state_input: bfloat16 [2, 2, 64, 64, 16], replicated, may hold values from -1.5 to 1.5
- state_output: float32 [2, 2, 64, 16, 64], replicated, may hold values from -0.375 to 0.375
- forget_rate: float32 [2, 64, 64], replicated, may hold values from 0 to 1, as said below
- decay_angle: float32 [2, 64, 64], replicated, may hold values from -3.140625 to 3.140625
- skip_gain: float32 [1024], replicated, may hold values from -4 to 4
- glu_weight: bfloat16 [1024, 1024], replicated, may hold values from -0.1875 to 0.1875
- glu_bias: float32 [1024], replicated, may hold values from -4 to 4
- out_weight: bfloat16 [1024, 2048], replicated, may hold values from -0.1875 to 0.1875
- out_gain: float32 [2048], replicated, may hold values from 0.1 to 1.9
Outputs:
- mixed: bfloat16 [4096, 2048], P(('sp', 'tp'))
Inputs may be any that keep to these rules, and one draw needn't show every extreme that they name: `elapsed`: positive time steps. `forget_rate`: positive rates.
All inputs are finite; a program needn't handle non-finite values.
Results may differ from a plain program's by a relative error of at most 0.0067.
Values sent between devices are 32-bit elements; how exact they have to be, the bound alone decides.
A program may use at most 128 MiB of HBM per device.

v0:
```python
import jax
import jax.numpy as jnp
from jax import lax
from jax.sharding import PartitionSpec as P

span_len = 16
epsilon = 1e-06


def entering_2(value, axis, combine, identity, reverse):
    size, here = (lax.axis_size(axis), lax.axis_index(axis))
    everything = jax.tree.map(lambda part: lax.all_gather(part, axis), value)
    start = jax.tree.map(
        lambda part, zero: jnp.broadcast_to(jnp.asarray(zero, part.dtype), part.shape),
        value,
        identity,
    )

    def turn(k, before):
        at = size - 1 - k if reverse else k
        reached = at > here if reverse else at < here
        new = combine(before, jax.tree.map(lambda part: part[at], everything))
        return jax.tree.map(lambda a, b: jnp.where(reached, a, b), new, before)

    return lax.fori_loop(0, size, turn, start)


def rms_scale(activations, gain_row):
    values = activations.astype(jnp.float32)
    return (
        values * lax.rsqrt(jnp.mean(values * values, axis=-1, keepdims=True) + epsilon) * gain_row
    )


def complex_times(a_re, a_im, b_re, b_im):
    return (a_re * b_re - a_im * b_im, a_re * b_im + a_im * b_re)


def link_pair(earlier, later):
    left_dr, left_di, left_sr, left_si = earlier
    right_dr, right_di, right_sr, right_si = later
    joint_re, joint_im = complex_times(left_dr, left_di, right_dr, right_di)
    moved_re, moved_im = complex_times(right_dr, right_di, left_sr, left_si)
    return (joint_re, joint_im, moved_re + right_sr, moved_im + right_si)


def read_out(state_re, state_im, readout):
    count = state_re.shape[0]
    groups, group_width, states = (readout.shape[1], readout.shape[2], readout.shape[3])
    real_part = jnp.einsum(
        "tgp,ghp->tgh",
        state_re.reshape(count, groups, states),
        readout[0],
        precision=lax.Precision.HIGHEST,
    )
    imag_part = jnp.einsum(
        "tgp,ghp->tgh",
        state_im.reshape(count, groups, states),
        readout[1],
        precision=lax.Precision.HIGHEST,
    )
    return (real_part - imag_part).reshape(count, groups * group_width)


def shifted(values, filler, backward):
    if backward:
        return jnp.concatenate([values[1:], filler], axis=0)
    return jnp.concatenate([filler, values[:-1]], axis=0)


def enter_state(total_steps, device_state, rate, angle, backward):
    cell_count = rate.shape[0]
    zero_col = jnp.zeros((cell_count,), jnp.float32)

    def merge_span(earlier, later):
        left_time, left_re, left_im = earlier
        right_time, right_re, right_im = later
        fade = jnp.exp(-rate * right_time)
        turn = angle * right_time
        moved_re, moved_im = complex_times(
            fade * jnp.cos(turn), fade * jnp.sin(turn), left_re, left_im
        )
        return (left_time + right_time, moved_re + right_re, moved_im + right_im)

    operand = (total_steps, device_state[0], device_state[1])
    identity = (jnp.zeros((), jnp.float32), zero_col, zero_col)
    if backward:
        entering = entering_2(operand, ("sp", "tp"), merge_span, identity, True)
    else:
        entering = entering_2(operand, ("sp", "tp"), merge_span, identity, False)
    return (entering[1], entering[2])


def one_direction(driven, elapsed, inputs, readout, rate, angle, backward):
    row_count = driven.shape[0]
    groups, states, group_width = (inputs.shape[1], inputs.shape[2], inputs.shape[3])
    cell_count = groups * states
    span_count = row_count // span_len
    grouped = driven.reshape(row_count, groups, group_width)
    proj_re = jnp.einsum(
        "tgh,gph->tgp", grouped, inputs[0], preferred_element_type=jnp.float32
    ).reshape(row_count, cell_count)
    proj_im = jnp.einsum(
        "tgh,gph->tgp", grouped, inputs[1], preferred_element_type=jnp.float32
    ).reshape(row_count, cell_count)
    steps_col = elapsed[:, None]
    damping = jnp.sqrt(-jnp.expm1(-2.0 * rate * steps_col))
    drive_re = proj_re * damping
    drive_im = proj_im * damping
    pieces = elapsed.reshape(span_count, span_len)
    if backward:
        within = jnp.cumsum(pieces[:, ::-1], axis=1)[:, ::-1]
        edge_index = 0
        last_index = 0
    else:
        within = jnp.cumsum(pieces, axis=1)
        edge_index = span_len - 1
        last_index = span_count - 1
    offset = within.reshape(row_count, 1)
    angles = angle * offset
    cosine = jnp.cos(angles)
    sine_part = jnp.sin(angles)
    growth = jnp.exp(rate * offset)
    shrink = jnp.exp(-rate * offset)
    lift_re, lift_im = complex_times(growth * cosine, -growth * sine_part, drive_re, drive_im)
    row_index = lax.broadcasted_iota(jnp.int32, (span_len, span_len), 0)
    col_index = lax.broadcasted_iota(jnp.int32, (span_len, span_len), 1)
    if backward:
        triangle = (row_index <= col_index).astype(jnp.float32)
    else:
        triangle = (row_index >= col_index).astype(jnp.float32)
    stacked = jnp.stack([lift_re, lift_im]).reshape(2, span_count, span_len, cell_count)
    partial_value = jnp.einsum(
        "ji,skic->skjc", triangle, stacked, precision=lax.Precision.HIGHEST
    ).reshape(2, row_count, cell_count)
    back_re = shrink * cosine
    back_im = shrink * sine_part
    local_re, local_im = complex_times(back_re, back_im, partial_value[0], partial_value[1])
    spread_re = back_re.reshape(span_count, span_len, cell_count)
    spread_im = back_im.reshape(span_count, span_len, cell_count)
    block_items = (
        spread_re[:, edge_index],
        spread_im[:, edge_index],
        local_re.reshape(span_count, span_len, cell_count)[:, edge_index],
        local_im.reshape(span_count, span_len, cell_count)[:, edge_index],
    )
    inclusive = lax.associative_scan(link_pair, block_items, axis=0, reverse=backward)
    unit_col = jnp.ones((1, cell_count), jnp.float32)
    zero_col = jnp.zeros((1, cell_count), jnp.float32)
    fade_re = shifted(inclusive[0], unit_col, backward)
    fade_im = shifted(inclusive[1], zero_col, backward)
    carry_re = shifted(inclusive[2], zero_col, backward)
    carry_im = shifted(inclusive[3], zero_col, backward)
    device_state = (inclusive[2][last_index], inclusive[3][last_index])
    total_steps = jnp.sum(elapsed)
    enter_re, enter_im = enter_state(total_steps, device_state, rate, angle, backward)
    pass_re, pass_im = complex_times(fade_re, fade_im, enter_re[None, :], enter_im[None, :])
    near_re, near_im = complex_times(
        spread_re, spread_im, (carry_re + pass_re)[:, None, :], (carry_im + pass_im)[:, None, :]
    )
    near_re, near_im = (
        near_re.reshape(row_count, cell_count),
        near_im.reshape(row_count, cell_count),
    )
    return read_out(local_re + near_re, local_im + near_im, readout)


def local(
    tokens,
    elapsed,
    norm_gain,
    in_weight,
    state_input,
    state_output,
    forget_rate,
    decay_angle,
    skip_gain,
    glu_weight,
    glu_bias,
    out_weight,
    out_gain,
):
    normed = rms_scale(tokens, norm_gain).astype(jnp.bfloat16)
    driven = jnp.dot(normed, in_weight, preferred_element_type=jnp.float32).astype(jnp.bfloat16)
    response = skip_gain * driven.astype(jnp.float32)
    for direction in range(2):
        response = response + one_direction(
            driven,
            elapsed,
            state_input[direction],
            state_output[direction],
            forget_rate[direction].reshape(-1),
            decay_angle[direction].reshape(-1),
            direction == 1,
        )
    active = jax.nn.gelu(response)
    gate_pre = (
        jnp.dot(active.astype(jnp.bfloat16), glu_weight, preferred_element_type=jnp.float32)
        + glu_bias
    )
    gated = (active * jax.nn.sigmoid(gate_pre)).astype(jnp.bfloat16)
    projected = jnp.dot(gated, out_weight, preferred_element_type=jnp.float32)
    return rms_scale(projected, out_gain).astype(jnp.bfloat16)


def solution(mesh):
    return jax.shard_map(
        local,
        mesh=mesh,
        in_specs=(
            P(("sp", "tp"), None),
            P(("sp", "tp")),
            P(),
            P(),
            P(),
            P(),
            P(),
            P(),
            P(),
            P(),
            P(),
            P(),
            P(),
        ),
        out_specs=P(("sp", "tp"), None),
        check_vma=False,
    )
```

profile of v0, /device:TPU:0, one launch (start us, length us, event | category | flops | bytes accessed | tf_op | source)
XLA Modules:
  0.0 661.2 jit_solution(125747833568181692)
XLA Ops:
  3.4 41.9 %all-reduce.56 = f32[32]{0:T(128)} all-reduce(f32[32]{0:T(128)S(1)} %dynamic-update-slice), channel_id=1, replica_groups=mesh['sp'=8,'tp'=4] {'sp','tp'}, use_global_device_ids=true, to_apply=%add.56 | all-reduce | flops 32 | bytes 256
  53.4 3.9 convolution_convert_fusion
  58.4 1.9 convolution_bitcast_fusion.2
  60.3 5.6 copy.78
  65.9 4.8 reshape.902
  70.7 1.9 convolution_bitcast_fusion.3
  72.6 5.6 copy.77
  78.2 4.8 reshape.901
  83.0 1.9 convolution_bitcast_fusion.4
  84.9 1.8 convolution_bitcast_fusion.5
  86.7 5.6 copy.66
  92.3 4.8 reshape.898
  97.1 5.6 copy.67
  102.7 4.8 reshape.899
  107.6 20.8 %multiply_subtract_fusion.1 = (f32[1,8,16,4096]{3,2,1,0:T(8,128)S(1)}, f32[1,8,16,4096]{3,2,1,0:T(8,128)S(1)}, f32[1,8,16,4096]{3,2,1,0:T(8,128)S(1)}, f32[1,8,16,4096]{3,2,1,0:T(8,128)S(1)}) fusion(f32[1,8,16,4096]{3,2,1,0:T(8,128)} %reshape.898, f32[1,8,16,4096]{3,2,1,0:T(8,128)} %reshape.899, f32[8,16]{1,0:T(8,128)S(1)} %copy-done.23, ...), kind=kLoop, calls=%fused_computation.79 | loop fusion | flops 15728640 | bytes 16877056 | tf_op jit(solution)/shard_map/sub | solution.py:36
  128.5 4.5 convolution_bitcast_fusion.1
  133.0 2.6 convolution_bitcast_fusion
  135.6 3.4 fusion.114
  139.6 4.6 squeeze.144
  144.2 4.7 squeeze.143
  148.8 10.7 %fusion.33 = (f32[8,16,4096]{2,0,1:T(8,128)S(1)}, f32[8,16,4096]{2,0,1:T(8,128)S(1)}, f32[8,16,4096]{2,0,1:T(8,128)S(1)}, f32[8,16,4096]{2,0,1:T(8,128)S(1)}) fusion(f32[1,8,16,4096]{3,2,1,0:T(8,128)} %get-tuple-element.562, f32[4096]{0:T(1024)S(1)} %mul.1358, f32[8,16]{0,1:T(8,128)S(1)} %copy-done.27, f32[4096]{0:T(1024)S(1)} %get-tuple-element.788, ...), kind=kLoop, calls=%fused_computation.85 | loop fusion | flops 4194304 | bytes 12616192 | tf_op jit(solution)/shard_map/mul | solution.py:36
  159.6 2.5 copy_add_fusion
  176.3 9.6 %slice.679 = f32[7,4096]{1,0:T(8,128)} reverse(f32[7,4096]{1,0:T(8,128)S(1)} %slice_add_fusion.22), dimensions={0} | reverse | bytes 229376 | tf_op jit(solution)/shard_map/slice | solution.py:67
  185.9 9.5 %slice.689 = f32[7,4096]{1,0:T(8,128)} reverse(f32[7,4096]{1,0:T(8,128)S(1)} %slice_add_fusion.23), dimensions={0} | reverse | bytes 229376 | tf_op jit(solution)/shard_map/slice | solution.py:67
  195.5 9.5 %slice.691 = f32[7,4096]{1,0:T(8,128)} reverse(f32[7,4096]{1,0:T(8,128)S(1)} %slice_add_fusion.21), dimensions={0} | reverse | bytes 229376 | tf_op jit(solution)/shard_map/slice | solution.py:67
  206.6 9.6 %slice.667 = f32[7,4096]{1,0:T(8,128)} reverse(f32[7,4096]{1,0:T(8,128)S(1)} %slice_add_fusion), dimensions={0} | reverse | bytes 229376 | tf_op jit(solution)/shard_map/slice | solution.py:67
  216.1 41.8 %all-gather.3 = f32[32,1,4096]{2,1,0:T(1,128)S(1)} all-gather(f32[1,1,4096]{2,1,0:T(1,128)S(1)} %add_bitcast_fusion), channel_id=1, replica_groups=mesh['sp'=8,'tp'=4] {'sp','tp'}, dimensions={0}, use_global_device_ids=true | all-gather | bytes 540672 | tf_op jit(solution)/shard_map/all_gather | solution.py:12
  258.2 5.3 fusion.113
  263.6 5.1 squeeze.132
  268.6 4.6 squeeze.131
  273.3 10.5 %fusion.32 = (f32[8,16,4096]{2,0,1:T(8,128)S(1)}, f32[8,16,4096]{2,0,1:T(8,128)S(1)}, f32[8,16,4096]{2,0,1:T(8,128)S(1)}, f32[8,16,4096]{2,0,1:T(8,128)S(1)}) fusion(f32[1,8,16,4096]{3,2,1,0:T(8,128)} %get-tuple-element.559, f32[4096]{0:T(1024)S(1)} %mul.1260, f32[8,16]{0,1:T(8,128)S(1)} %copy-done.26, f32[4096]{0:T(1024)S(1)} %get-tuple-element.827, ...), kind=kLoop, calls=%fused_computation.84 | loop fusion | flops 4194304 | bytes 12616192 | tf_op jit(solution)/shard_map/mul | solution.py:36
  283.8 2.5 copy_add_fusion.1
  308.8 38.0 %all-gather = f32[32,1,4096]{2,1,0:T(1,128)S(1)} all-gather(f32[1,1,4096]{2,1,0:T(1,128)S(1)} %get-tuple-element.645), channel_id=1, replica_groups=mesh['sp'=8,'tp'=4] {'sp','tp'}, dimensions={0}, use_global_device_ids=true | all-gather | bytes 540672 | tf_op jit(solution)/shard_map/all_gather | solution.py:12
  347.1 39.6 %all-gather.1 = f32[32,1,4096]{2,1,0:T(1,128)S(1)} all-gather(f32[1,1,4096]{2,1,0:T(1,128)S(1)} %add_bitcast_fusion.1), channel_id=1, replica_groups=mesh['sp'=8,'tp'=4] {'sp','tp'}, dimensions={0}, use_global_device_ids=true | all-gather | bytes 540672 | tf_op jit(solution)/shard_map/all_gather | solution.py:12
  387.8 76.8 %while.36 = (s32[]{:T(128)}, f32[4096]{0:T(1024)S(1)}, f32[4096]{0:T(1024)S(1)}, s32[]{:T(128)}, f32[32]{0:T(128)S(1)}, /*index=5*/f32[4096]{0:T(1024)S(1)}, f32...) while((s32[]{:T(128)}, f32[4096]{0:T(1024)S(1)}, ...), condition=%wide.region_4.5_spmd.clone, body=%wide.region_3.4_spmd.clone.sunk | while | flops 65540 | bytes 196765 | solution.py:25
  465.8 38.1 %all-gather.2 = f32[32,1,4096]{2,1,0:T(1,128)S(1)} all-gather(f32[1,1,4096]{2,1,0:T(1,128)S(1)} %get-tuple-element.646), channel_id=1, replica_groups=mesh['sp'=8,'tp'=4] {'sp','tp'}, dimensions={0}, use_global_device_ids=true | all-gather | bytes 540672 | tf_op jit(solution)/shard_map/all_gather | solution.py:12
  504.2 44.2 %while.37 = (s32[]{:T(128)}, f32[4096]{0:T(1024)S(1)}, f32[4096]{0:T(1024)S(1)}, s32[]{:T(128)}, f32[32]{0:T(128)S(1)}, /*index=5*/f32[4096]{0:T(1024)S(1)}, f32...) while((s32[]{:T(128)}, f32[4096]{0:T(1024)S(1)}, ...), condition=%wide.region_7.8_spmd.clone, body=%wide.region_6.7_spmd.clone.sunk | while | flops 65544 | bytes 196827 | solution.py:25
  552.8 4.6 mul.1340
  557.4 4.7 mul.1436
  563.6 4.6 mul.1431
  569.8 4.7 mul.1335
  574.5 38.9 %subtract_add_fusion = (f32[128,64,64]{2,1,0:T(8,128)S(1)}, f32[128,64,64]{2,1,0:T(8,128)S(1)}, f32[128,64,64]{2,1,0:T(8,128)}, f32[128,64,64]{2,1,0:T(8,128)}) fusion(f32[128,64,64]{2,1,0:T(8,128)} %mul.1436, f32[128,64,64]{2,1,0:T(8,128)} %mul.1431, f32[128,64,64]{2,1,0:T(8,128)} %squeeze.144, f32[128,64,64]{2,1,0:T(8,128)} %squeeze.143, ...), kind=kLoop, calls=%fused_computation.39 | loop fusion | flops 18874368 | bytes 25232384 | tf_op jit(solution)/shard_map/add | solution.py:165
  613.4 8.8 %fusion.10 = f32[64,128,16]{1,2,0:T(8,128)S(1)} fusion(f32[128,64,64]{2,1,0:T(8,128)S(1)} %get-tuple-element.552, f32[2,2,64,16,64]{4,3,2,1,0:T(8,128)S(1)} %copy-done.5), kind=kOutput, calls=%fused_computation.30 | convolution fusion | flops 100663296 | bytes 5242880 | tf_op jit(solution)/shard_map/tgp,ghp->tgh/dot_general | solution.py:56
  622.3 9.1 %fusion.37 = f32[64,128,16]{1,2,0:T(8,128)S(1)} fusion(f32[64,128,16]{1,2,0:T(8,128)S(1)} %fusion.10, f32[128,64,64]{2,1,0:T(8,128)S(1)} %get-tuple-element.551, f32[2,2,64,16,64]{4,3,2,1,0:T(8,128)S(1)} %copy-done.5), kind=kOutput, calls=%fused_computation.93 | convolution fusion | flops 100794368 | bytes 5767168 | tf_op jit(solution)/shard_map/tgp,ghp->tgh/dot_general | solution.py:50
  631.6 11.0 %fusion.14 = f32[64,128,16]{1,2,0:T(8,128)S(1)} fusion(f32[128,64,64]{2,1,0:T(8,128)} %get-tuple-element.655, f32[2,2,64,16,64]{4,3,2,1,0:T(8,128)} %param.22), kind=kOutput, calls=%fused_computation.34 | convolution fusion | flops 100663296 | bytes 5242880 | tf_op jit(solution)/shard_map/tgp,ghp->tgh/dot_general | solution.py:56
  642.6 9.9 %fusion.34 = f32[64,128,16]{1,2,0:T(8,128)S(1)} fusion(f32[64,128,16]{1,2,0:T(8,128)S(1)} %fusion.14, f32[128,64,64]{2,1,0:T(8,128)S(1)} %copy-done.4, f32[2,2,64,16,64]{4,3,2,1,0:T(8,128)} %param.22), kind=kOutput, calls=%fused_computation.92 | convolution fusion | flops 100794368 | bytes 3670016 | tf_op jit(solution)/shard_map/tgp,ghp->tgh/dot_general | solution.py:50
  653.6 5.0 multiply_reduce_fusion
  658.6 2.2 multiply_convert_fusion
  (471 shorter events, 181.4 us)
Async XLA Ops:
  0.0 653.6 %copy-start = (bf16[1024,1024]{1,0:T(8,128)(2,1)S(1)}, bf16[1024,1024]{1,0:T(8,128)(2,1)}, u32[]{:S(2)}) copy-start(bf16[1024,1024]{1,0:T(8,128)(2,1)} %param.26) | copy-start | bytes 6291460
  46.1 0.8 copy-start.22
  46.2 2.8 copy-start.18
  47.1 1.9 copy-start.20
  53.4 5.0 copy-start.6
  102.7 4.9 copy-start.19
  102.7 4.9 copy-start.21
  102.7 4.9 copy-start.23
  102.7 4.9 copy-start.24
  102.7 4.9 copy-start.25
  135.6 4.0 copy-start.2
  144.2 4.7 copy-start.27
  148.8 10.7 %copy-start.3 = (f32[2,8,16,4096]{3,2,1,0:T(8,128)S(1)}, f32[2,8,16,4096]{3,2,1,0:T(8,128)}, u32[]{:S(2)}) copy-start(f32[2,8,16,4096]{3,2,1,0:T(8,128)} %copy-done.2) | copy-start | bytes 12582916
  268.6 4.6 copy-start.26
  273.3 10.5 %copy-start.1 = (f32[2,8,16,4096]{3,2,1,0:T(8,128)S(1)}, f32[2,8,16,4096]{3,2,1,0:T(8,128)}, u32[]{:S(2)}) copy-start(f32[2,8,16,4096]{3,2,1,0:T(8,128)} %convolution_bitcast_fusion.1) | copy-start | bytes 12582916
  289.2 9.9 %copy-start.8 = (f32[3,4096]{1,0:T(4,128)}, f32[3,4096]{1,0:T(4,128)S(1)}, u32[]{:S(2)}) copy-start(f32[3,4096]{1,0:T(4,128)S(1)} %slice.580) | copy-start | bytes 147460
  296.0 1.1 copy-start.12
  296.0 1.2 copy-start.13
  307.0 80.8 %copy-start.10 = (f32[4096]{0:T(1024)S(1)}, f32[4096]{0:T(1024)}, u32[]{:S(2)}) copy-start(f32[4096]{0:T(1024)} %custom-call.1) | copy-start | bytes 49156
  307.0 80.8 %copy-start.11 = (f32[4096]{0:T(1024)S(1)}, f32[4096]{0:T(1024)}, u32[]{:S(2)}) copy-start(f32[4096]{0:T(1024)} %custom-call) | copy-start | bytes 49156
  307.0 80.8 %copy-start.33 = (f32[32]{0:T(128)S(1)}, f32[32]{0:T(128)}, u32[]{:S(2)}) copy-start(f32[32]{0:T(128)} %all-reduce.56) | copy-start | bytes 388
  387.8 116.4 %copy-start.9 = (f32[4096]{0:T(1024)S(1)}, f32[4096]{0:T(1024)}, u32[]{:S(2)}) copy-start(f32[4096]{0:T(1024)} %custom-call.2) | copy-start | bytes 49156
  464.6 39.6 %copy-start.34 = (f32[32]{0:T(128)S(1)}, f32[32]{0:T(128)}, u32[]{:S(2)}) copy-start(f32[32]{0:T(128)} %all-reduce.56) | copy-start | bytes 388
  569.8 4.7 copy-start.14
  569.8 4.7 copy-start.15
  569.8 4.7 copy-start.16
  569.8 4.7 copy-start.17
  569.8 4.7 copy-start.29
  569.8 4.7 copy-start.30
  574.5 38.9 %copy-start.5 = (f32[2,2,64,16,64]{4,3,2,1,0:T(8,128)S(1)}, f32[2,2,64,16,64]{4,3,2,1,0:T(8,128)}, u32[]{:S(2)}) copy-start(f32[2,2,64,16,64]{4,3,2,1,0:T(8,128)} %param.22) | copy-start | bytes 3145732
  631.6 11.0 %copy-start.4 = (f32[128,64,64]{2,1,0:T(8,128)S(1)}, f32[128,64,64]{2,1,0:T(8,128)}, u32[]{:S(2)}) copy-start(f32[128,64,64]{2,1,0:T(8,128)} %get-tuple-element.656) | copy-start | bytes 6291460
  642.6 11.0 %copy-start.7 = (bf16[128,1024]{1,0:T(8,128)(2,1)S(1)}, bf16[128,1024]{1,0:T(8,128)(2,1)}, u32[]{:S(2)}) copy-start(bf16[128,1024]{1,0:T(8,128)(2,1)} %convolution_convert_fusion) | copy-start | bytes 786436
  642.6 11.0 %copy-start.31 = (f32[1024]{0:T(1024)S(1)}, f32[1024]{0:T(1024)}, u32[]{:S(2)}) copy-start(f32[1024]{0:T(1024)} %param.27) | copy-start | bytes 12292
  642.6 11.0 %copy-start.32 = (f32[1024]{0:T(1024)S(1)}, f32[1024]{0:T(1024)}, u32[]{:S(2)}) copy-start(f32[1024]{0:T(1024)} %param.25) | copy-start | bytes 12292
  653.6 5.0 copy-start.28
where the time goes:
time: 673 us; the launch traced here: 661 us
  local copies, waits for them, and re-layouts  237 us (35%)
  blocking collectives  199 us (30%)
  other arithmetic  158 us (23%)
  matrix products  62.3 us (9%)
    all_gather x4, blocking collectives, entering_2(): everything = jax.tree.map(lambda part: lax.all_gather(part, axis), value)  158 us
    dynamic_slice x128, local copies, waits for them, and re-layouts, turn(): new = combine(before, jax.tree.map(lambda part: part[at], everything))  70.7 us
    select_n x64, other arithmetic, turn(): return jax.tree.map(lambda a, b: jnp.where(reached, a, b), new, before)  48.3 us
    unnamed x1, blocking collectives  41.9 us
    add x1, other arithmetic, one_direction(): return read_out(local_re + near_re, local_im + near_im, readout)  38.9 us
    slice x7, local copies, waits for them, and re-layouts, shifted(): return jnp.concatenate([values[1:], filler], axis=0)  38.3 us
    mul x8, local copies, waits for them, and re-layouts, complex_times(): return (a_re * b_re - a_im * b_im, a_re * b_im + a_im * b_re)  24.8 us
    sub x3, other arithmetic, complex_times(): return (a_re * b_re - a_im * b_im, a_re * b_im + a_im * b_re)  21.8 us

commit v1 on v0

v1 whole, which is shorter than its diff:
```python
import functools
import math

import jax
import jax.numpy as jnp
from jax import lax
from jax.experimental import pallas as pl
from jax.experimental.pallas import tpu as pltpu
from jax.sharding import PartitionSpec as P

epsilon = 1e-06
LANES = 128
SUB = 8
SIN = (4.44288292, -7.30824569, 3.60635422, -0.84611165, 0.10982452)
COS = (1.41421356, -6.97886411, 5.73988154, -1.88827492, 0.33225154, -0.03450161)
F32 = jnp.float32
BF16 = jnp.bfloat16


def horner(coefs, z):
    total = jnp.full_like(z, coefs[-1])
    for coef in coefs[-2::-1]:
        total = total * z + coef
    return total


def cos_sin(turns):
    part = turns - jnp.round(turns)
    square = part * part
    half_sin = part * horner(SIN, square)
    half_cos = horner(COS, square)
    return 1.0 - half_sin * half_sin, half_sin * half_cos


def one_less_exp(y, fade):
    series = y * horner((1.0, -1 / 2, 1 / 6, -1 / 24, 1 / 120, -1 / 720), y)
    return jnp.where(y < 0.4, series, 1.0 - fade * fade)


def cmul(a, b):
    return a[0] * b[0] - a[1] * b[1], a[0] * b[1] + a[1] * b[0]


def decay_of(rate, angle, time):
    fade = jnp.exp2(time * (rate * (-math.log2(math.e))))
    cosine, sine = cos_sin(time * (angle * (0.5 / math.pi)))
    return fade * cosine, fade * sine


def kernel(
    sp_size, tp_size,
    tokens_ref, elapsed_ref, norm_ref, drive_ref, read_ref, rate_ref, angle_ref,
    skip_ref, bias_ref, gain_ref, in_hbm, glu_hbm, out_hbm,
    mixed_ref,
    in_ref, glu_ref, out_ref, e_ref, driven_ref, proj_ref, sre, sim, pre, pim,
    ends, segs, st_ref, resp_ref,
    send1, recv1, send2, recv2, send3, recv3,
    wsem, s1s, r1s, s2s, r2s, s3s, r3s,
):
    rows = tokens_ref.shape[0]
    steps = rows // SUB
    pairs = rate_ref.shape[1]
    per = pairs // tp_size
    blocks = driven_ref.shape[1] // LANES
    inner = pairs // blocks
    wide = LANES // inner
    my_sp, my_tp = lax.axis_index("sp"), lax.axis_index("tp")

    loads = [
        pltpu.make_async_copy(a, b, wsem.at[i])
        for i, (a, b) in enumerate(((in_hbm, in_ref), (glu_hbm, glu_ref), (out_hbm, out_ref)))
    ]
    for load in loads:
        load.start()
    barrier = pltpu.get_barrier_semaphore()
    for off in range(1, tp_size):
        pl.semaphore_signal(
            barrier, inc=1, device_id=(my_sp, lax.rem(my_tp + off, tp_size)),
            device_id_type=pl.DeviceIdType.MESH,
        )
    for off in range(1, sp_size):
        pl.semaphore_signal(
            barrier, inc=1, device_id=(lax.rem(my_sp + off, sp_size), my_tp),
            device_id_type=pl.DeviceIdType.MESH,
        )

    at_row = lax.broadcasted_iota(jnp.int32, (rows, rows), 0)
    at_col = lax.broadcasted_iota(jnp.int32, (rows, rows), 1)
    place = at_col == (at_row & (SUB - 1)) * steps + (at_row >> 3)
    permute = place.astype(F32).astype(BF16)
    back = (at_row == (at_col & (SUB - 1)) * steps + (at_col >> 3)).astype(F32).astype(BF16)
    e_row = elapsed_ref[...]
    total_time = jnp.sum(e_row, axis=1, keepdims=True)
    e_ref[...] = jnp.broadcast_to(
        jnp.sum(jnp.where(place, e_row, 0.0), axis=1, keepdims=True), (rows, LANES)
    )

    values = tokens_ref[...].astype(F32)
    scale = lax.rsqrt(jnp.mean(values * values, axis=-1, keepdims=True) + epsilon)
    normed = (values * scale * norm_ref[...]).astype(BF16)
    loads[0].wait()
    driven = jnp.dot(normed, in_ref[...], preferred_element_type=F32).astype(BF16)
    driven_ref[...] = jnp.dot(permute, driven, preferred_element_type=F32).astype(BF16)

    lane = lax.broadcasted_iota(jnp.int32, (1, LANES), 1)

    def unit(k, r):
        rate = rate_ref[k, pl.ds(r, 1), :]
        twice = jnp.broadcast_to(rate * 2.0, (SUB, LANES))
        slope = jnp.broadcast_to(rate * (-math.log2(math.e)), (SUB, LANES))
        spin = jnp.broadcast_to(angle_ref[k, pl.ds(r, 1), :] * (0.5 / math.pi), (SUB, LANES))
        state = prod = None
        order = range(steps) if k == 0 else range(steps - 1, -1, -1)
        for j in order:
            at = slice(j * SUB, (j + 1) * SUB)
            e = e_ref[at, :]
            fade = jnp.exp2(e * slope)
            rise = one_less_exp(e * twice, fade)
            damping = rise * lax.rsqrt(jnp.maximum(rise, 1e-36))
            cosine, sine = cos_sin(e * spin)
            decay = (fade * cosine, fade * sine)
            push_re = proj_ref[at, k * 256 : k * 256 + 128] * damping
            push_im = proj_ref[at, k * 256 + 128 : k * 256 + 256] * damping
            if state is None:
                state, prod = (push_re, push_im), decay
            else:
                moved = cmul(decay, state)
                state = (moved[0] + push_re, moved[1] + push_im)
                prod = cmul(decay, prod)
            sre[k, r, at, :] = state[0]
            sim[k, r, at, :] = state[1]
            pre[k, r, at, :] = prod[0]
            pim[k, r, at, :] = prod[1]
        ends[k, 0, r] = state[0]
        ends[k, 1, r] = state[1]
        ends[k, 2, r] = prod[0]
        ends[k, 3, r] = prod[1]

    def block(b, carry):
        start = pl.multiple_of(b * LANES, LANES)
        piece = driven_ref[:, pl.ds(start, LANES)]
        weight = drive_ref[pl.ds(start, LANES), :]

        def one(i, carry):
            mask = (lane // wide == i).astype(F32).astype(BF16)
            proj_ref[...] = jnp.dot(piece * mask, weight, preferred_element_type=F32)
            unit(0, b * inner + i)
            unit(1, b * inner + i)
            return carry

        return lax.fori_loop(0, inner, one, carry)

    lax.fori_loop(0, blocks, block, 0)

    sub = lax.broadcasted_iota(jnp.int32, (per, SUB, LANES), 1)
    for q in range(tp_size):
        for k in range(2):
            at = slice(q * per, (q + 1) * per)
            s = (ends[k, 0, at], ends[k, 1, at])
            p = (ends[k, 2, at], ends[k, 3, at])

            def shift(x, far, fill):
                moved = pltpu.roll(x, far if k == 0 else SUB - far, 1)
                keep = sub >= far if k == 0 else sub < SUB - far
                return jnp.where(keep, moved, fill)

            for far in (1, 2, 4):
                old_s = (shift(s[0], far, 0.0), shift(s[1], far, 0.0))
                old_p = (shift(p[0], far, 1.0), shift(p[1], far, 0.0))
                moved = cmul(p, old_s)
                s = (moved[0] + s[0], moved[1] + s[1])
                p = cmul(p, old_p)
            last = SUB - 1 if k == 0 else 0
            send1[q, 2 * k] = s[0][:, last, :]
            send1[q, 2 * k + 1] = s[1][:, last, :]
            segs[k, 0, at] = shift(s[0], 1, 0.0)
            segs[k, 1, at] = shift(s[1], 1, 0.0)
            segs[k, 2, at] = shift(p[0], 1, 1.0)
            segs[k, 3, at] = shift(p[1], 1, 0.0)
        send1[q, 4] = jnp.broadcast_to(total_time, (per, LANES))

    pl.semaphore_wait(barrier, tp_size + sp_size - 2)

    def exchange_tp(send, recv, ssem, rsem):
        outs = []
        for off in range(1, tp_size):
            peer = lax.rem(my_tp + off, tp_size)
            copy = pltpu.make_async_remote_copy(
                src_ref=send.at[peer], dst_ref=recv.at[my_tp],
                send_sem=ssem.at[peer], recv_sem=rsem.at[my_tp],
                device_id=(my_sp, peer), device_id_type=pl.DeviceIdType.MESH,
            )
            copy.start()
            outs.append(copy)
        recv[my_tp] = send[my_tp]
        for off in range(1, tp_size):
            peer = lax.rem(my_tp + off, tp_size)
            pltpu.make_async_remote_copy(
                src_ref=send.at[peer], dst_ref=recv.at[peer],
                send_sem=ssem.at[peer], recv_sem=rsem.at[peer],
                device_id=(my_sp, peer), device_id_type=pl.DeviceIdType.MESH,
            ).wait_recv()
        return outs

    pending = exchange_tp(send1, recv1, s1s, r1s)
    mine = pl.ds(my_tp * per, per)
    rate = (rate_ref[0, mine, :], rate_ref[1, mine, :])
    angle = (angle_ref[0, mine, :], angle_ref[1, mine, :])
    fold = []
    for k in range(2):
        fold.append([decay_of(rate[k], angle[k], recv1[i, 4]) for i in range(tp_size)])
    group_time = recv1[0, 4]
    for i in range(1, tp_size):
        group_time = group_time + recv1[i, 4]
    for k in range(2):
        total = None
        for i in range(tp_size) if k == 0 else range(tp_size - 1, -1, -1):
            s = (recv1[i, 2 * k], recv1[i, 2 * k + 1])
            if total is None:
                total = s
            else:
                moved = cmul(fold[k][i], total)
                total = (moved[0] + s[0], moved[1] + s[1])
        send2[2 * k] = total[0]
        send2[2 * k + 1] = total[1]
    send2[4] = group_time

    for off in range(1, sp_size):
        peer = lax.rem(my_sp + off, sp_size)
        copy = pltpu.make_async_remote_copy(
            src_ref=send2, dst_ref=recv2.at[my_sp],
            send_sem=s2s.at[peer], recv_sem=r2s.at[my_sp],
            device_id=(peer, my_tp), device_id_type=pl.DeviceIdType.MESH,
        )
        copy.start()
        pending.append(copy)
    recv2[my_sp] = send2[...]
    for off in range(1, sp_size):
        peer = lax.rem(my_sp + off, sp_size)
        pltpu.make_async_remote_copy(
            src_ref=send2, dst_ref=recv2.at[peer],
            send_sem=s2s.at[peer], recv_sem=r2s.at[peer],
            device_id=(peer, my_tp), device_id_type=pl.DeviceIdType.MESH,
        ).wait_recv()

    for k in range(2):
        enter = (jnp.zeros((per, LANES), F32), jnp.zeros((per, LANES), F32))
        for i in range(sp_size) if k == 0 else range(sp_size - 1, -1, -1):
            moved = cmul(decay_of(rate[k], angle[k], recv2[i, 4]), enter)
            reached = (jnp.full((per, LANES), i, jnp.int32) < my_sp) if k == 0 else (
                jnp.full((per, LANES), i, jnp.int32) > my_sp
            )
            enter = tuple(
                jnp.where(reached, moved[c] + recv2[i, 2 * k + c], enter[c]) for c in range(2)
            )
        for i in range(tp_size) if k == 0 else range(tp_size - 1, -1, -1):
            send3[i, 2 * k] = enter[0]
            send3[i, 2 * k + 1] = enter[1]
            moved = cmul(fold[k][i], enter)
            enter = tuple(moved[c] + recv1[i, 2 * k + c] for c in range(2))
    pending = pending + exchange_tp(send3, recv3, s3s, r3s)

    def read_block(b, carry):
        start = pl.multiple_of(b * LANES, LANES)
        weight = read_ref[pl.ds(start, LANES), :]

        def one(i, total):
            r = b * inner + i
            q, row = r // per, lax.rem(r, per)
            for k in range(2):
                enter = (
                    recv3[q, 2 * k, pl.ds(row, 1), :],
                    recv3[q, 2 * k + 1, pl.ds(row, 1), :],
                )
                moved = cmul((segs[k, 2, r], segs[k, 3, r]), enter)
                enter = (moved[0] + segs[k, 0, r], moved[1] + segs[k, 1, r])
                shape = (steps, SUB, LANES)
                prod = (pre[k, r].reshape(shape), pim[k, r].reshape(shape))
                moved = cmul(prod, enter)
                whole_re = sre[k, r].reshape(shape) + moved[0]
                whole_im = sim[k, r].reshape(shape) + moved[1]
                st_ref[:, k * 256 : k * 256 + 128] = whole_re.reshape(rows, LANES).astype(BF16)
                st_ref[:, k * 256 + 128 : k * 256 + 256] = whole_im.reshape(rows, LANES).astype(BF16)
            out = lax.dot_general(
                st_ref[...], weight, (((1,), (1,)), ((), ())), preferred_element_type=F32
            )
            return jnp.where(lane // wide == i, out, total)

        resp_ref[:, pl.ds(start, LANES)] = lax.fori_loop(
            0, inner, one, jnp.zeros((rows, LANES), F32)
        )
        return carry

    lax.fori_loop(0, blocks, read_block, 0)

    response = resp_ref[...] + skip_ref[...] * driven_ref[...].astype(F32)
    active = jax.nn.gelu(response)
    loads[1].wait()
    gate = jnp.dot(active.astype(BF16), glu_ref[...], preferred_element_type=F32) + bias_ref[...]
    gated = (active * jax.nn.sigmoid(gate)).astype(BF16)
    gated = jnp.dot(back, gated, preferred_element_type=F32).astype(BF16)
    loads[2].wait()
    projected = jnp.dot(gated, out_ref[...], preferred_element_type=F32)
    scale = lax.rsqrt(jnp.mean(projected * projected, axis=-1, keepdims=True) + epsilon)
    mixed_ref[...] = (projected * scale * gain_ref[...]).astype(BF16)
    for copy in pending:
        copy.wait_send()


def local(
    sp_size, tp_size, tokens, elapsed, norm_gain, in_weight, state_input, state_output,
    forget_rate, decay_angle, skip_gain, glu_weight, glu_bias, out_weight, out_gain,
):
    rows, width = tokens.shape
    channels = in_weight.shape[1]
    _, _, groups, states, _ = state_input.shape
    share = LANES // states
    pairs = groups // share
    per = pairs // tp_size
    parity = (jnp.arange(groups)[:, None] % share == jnp.arange(share)[None, :])
    parity = parity[:, None, None, None, :, None]

    def spread(values):
        return jnp.where(parity, values[:, :, :, :, None, :], 0).astype(BF16).reshape(
            channels, 4 * LANES
        )

    drive = spread(state_input.transpose(2, 4, 0, 1, 3))
    sign = jnp.array([1.0, -1.0], F32)[None, :, None, None, None]
    read = spread((state_output * sign).transpose(2, 3, 0, 1, 4))

    vmem = pl.BlockSpec(memory_space=pltpu.VMEM)
    hbm = pl.BlockSpec(memory_space=pl.ANY)
    cells = (2, pairs, rows, LANES)
    dma = pltpu.SemaphoreType.DMA
    return pl.pallas_call(
        functools.partial(kernel, sp_size, tp_size),
        out_shape=jax.ShapeDtypeStruct((rows, width), BF16),
        in_specs=[vmem] * 10 + [hbm] * 3,
        out_specs=vmem,
        scratch_shapes=[
            pltpu.VMEM(in_weight.shape, BF16),
            pltpu.VMEM(glu_weight.shape, BF16),
            pltpu.VMEM(out_weight.shape, BF16),
            pltpu.VMEM((rows, LANES), F32),
            pltpu.VMEM((rows, channels), BF16),
            pltpu.VMEM((rows, 4 * LANES), F32),
            pltpu.VMEM(cells, F32),
            pltpu.VMEM(cells, F32),
            pltpu.VMEM(cells, F32),
            pltpu.VMEM(cells, F32),
            pltpu.VMEM((2, 4, pairs, SUB, LANES), F32),
            pltpu.VMEM((2, 4, pairs, SUB, LANES), F32),
            pltpu.VMEM((rows, 4 * LANES), BF16),
            pltpu.VMEM((rows, channels), F32),
            pltpu.VMEM((tp_size, 5, per, LANES), F32),
            pltpu.VMEM((tp_size, 5, per, LANES), F32),
            pltpu.VMEM((5, per, LANES), F32),
            pltpu.VMEM((sp_size, 5, per, LANES), F32),
            pltpu.VMEM((tp_size, 4, per, LANES), F32),
            pltpu.VMEM((tp_size, 4, per, LANES), F32),
            dma((3,)),
            dma((tp_size,)),
            dma((tp_size,)),
            dma((sp_size,)),
            dma((sp_size,)),
            dma((tp_size,)),
            dma((tp_size,)),
        ],
        compiler_params=pltpu.CompilerParams(
            collective_id=0, has_side_effects=True, vmem_limit_bytes=60 * 1024 * 1024
        ),
    )(
        tokens, elapsed.reshape(1, rows), norm_gain.reshape(1, -1), drive, read,
        forget_rate.reshape(2, pairs, LANES), decay_angle.reshape(2, pairs, LANES),
        skip_gain.reshape(1, -1), glu_bias.reshape(1, -1), out_gain.reshape(1, -1),
        in_weight, glu_weight, out_weight,
    )


def solution(mesh):
    rows = P(("sp", "tp"), None)
    return jax.shard_map(
        functools.partial(local, mesh.shape["sp"], mesh.shape["tp"]),
        mesh=mesh,
        in_specs=(rows, P(("sp", "tp"))) + (P(),) * 11,
        out_specs=rows,
        check_vma=False,
    )
```

time: 673 us -> 62.2 us (0.09); the launches traced: 661 us -> 62 us
  local copies, waits for them, and re-layouts: 237 us -> 13.4 us
  blocking collectives: 199 us -> 0 us
  other arithmetic: 158 us -> 7.92 us
  matrix products: 62.3 us -> 0 us
  Pallas kernels: 0 us -> 40.6 us
    all_gather x4 -> x0, blocking collectives: 158 us -> none  [entering_2(): everything = jax.tree.map(lambda part: lax.all_gather(part, axis), value)]
    dynamic_slice x128 -> x0, local copies, waits for them, and re-layouts: 70.7 us -> none  [turn(): new = combine(before, jax.tree.map(lambda part: part[at], everything))]
    slice x80 -> x0, local copies, waits for them, and re-layouts: 66.5 us -> none  [the longest x7 38.3 us: shifted(): return jnp.concatenate([values[1:], filler], axis=0)]
    dot_general x12 -> x0, matrix products: 62.3 us -> none  [the longest x2 19.8 us: read_out(): jnp.einsum('tgp,ghp->tgh', state_im.reshape(count, groups, states), reado...]
    add x41 -> x0, other arithmetic: 54 us -> none  [the longest x1 38.9 us: one_direction(): return read_out(local_re + near_re, local_im + near_im, readout)]
    select_n x64 -> x1, other arithmetic: 48.3 us -> 0.01 us  [local(): parity = jnp.arange(groups)[:, None] % share == jnp.arange(share)[None, :]]
    unnamed x1 -> x0, blocking collectives: 41.9 us -> none
    pallas_call x0 -> x1, Pallas kernels: none -> 40.6 us  [local(): pl.pallas_call(functools.partial(kernel, sp_size, tp_size), out_shape=jax...]
where the time goes in v1:
time: 62.2 us; the launch traced here: 62 us
  Pallas kernels  40.6 us (65%)
  local copies, waits for them, and re-layouts  13.4 us (22%)
  other arithmetic  7.92 us (13%)
    pallas_call x1, Pallas kernels, local(): pl.pallas_call(functools.partial(kernel, sp_size, tp_size), out_shape=jax...  40.6 us
    convert_element_type x1, local copies, waits for them, and re-layouts, spread(): jnp.where(parity, values[:, :, :, :, None, :], 0).astype(BF16)  5.98 us
    convert_element_type x1, other arithmetic, spread(): jnp.where(parity, values[:, :, :, :, None, :], 0).astype(BF16)  5.92 us
    select_n x1, local copies, waits for them, and re-layouts, spread(): jnp.where(parity, values[:, :, :, :, None, :], 0).astype(BF16)  2.02 us
    transpose x1, other arithmetic, local(): read = spread((state_output * sign).transpose(2, 3, 0, 1, 4))  1.92 us
    unnamed x7, local copies, waits for them, and re-layouts  1.89 us

profile of v1, /device:TPU:0, one launch (start us, length us, event | category | flops | bytes accessed | tf_op | source)
XLA Modules:
  0.0 62.0 jit_solution(16544769740760460849)
XLA Ops:
  0.0 0.0 copy-start
  0.0 1.9 %multiply_bitcast_fusion = bf16[64,16,2,2,64]{4,1,0,3,2:T(8,128)(2,1)S(1)} fusion(f32[2,2,64,16,64]{4,3,2,1,0:T(8,128)} %param.19, f32[2]{0:T(128)} %constant.23.clone), kind=kLoop, calls=%fused_computation.2 | loop fusion | flops 524288 | bytes 1572872 | tf_op jit(solution)/shard_map/transpose | solution.py:330
  1.9 1.1 %copy.16 = bf16[64,16,2,2,64]{4,3,2,1,0:T(2,128)(2,1)S(1)} copy(bf16[64,16,2,2,64]{4,1,0,3,2:T(8,128)(2,1)S(1)} %multiply_bitcast_fusion) | data formatting | bytes 1048576 | tf_op jit(solution)/shard_map/transpose | solution.py:330
  3.0 0.0 copy-done
  3.0 1.1 %copy.15 = bf16[64,16,2,2,64]{4,3,2,1,0:T(2,128)(2,1)S(1)} copy(bf16[64,16,2,2,64]{4,1,0,3,2:T(8,128)(2,1)S(1)} %bitcast.8) | data formatting | bytes 1048576 | tf_op jit(solution)/shard_map/transpose | solution.py:328
  4.1 0.1 iota_compare_fusion
  4.2 5.9 %select_convert_fusion = (bf16[64,16,2,2,2,64]{5,4,3,2,1,0:T(2,128)(2,1)}, bf16[64,16,2,2,2,64]{5,4,3,2,1,0:T(2,128)(2,1)S(1)}) fusion(pred[64,2]{1,0:T(8,128)(4,1)S(1)} %iota_compare_fusion, bf16[64,16,2,2,64]{4,3,2,1,0:T(2,128)(2,1)S(1)} %copy.16, bf16[64,16,2,2,64]{4,3,2,1,0:T(2,128)(2,1)S(1)} %copy.15), kind=kLoop, calls=%fused_computation | loop fusion | flops 1048576 | bytes 3145856 | tf_op jit(solution)/shard_map/convert_element_type | solution.py:324
  10.1 6.0 %convert_element_type.12.read_ref = bf16[1024,512]{1,0:T(8,128)(2,1)} reshape(bf16[64,16,2,2,2,64]{5,4,3,2,1,0:T(2,128)(2,1)} %get-tuple-element.5) | data formatting | bytes 2097152 | tf_op jit(solution)/shard_map/convert_element_type | solution.py:324
  16.1 0.0 copy-start.1
  16.1 0.0 copy-start.2
  16.1 2.0 %select_n.30.drive_ref = bf16[1024,512]{1,0:T(8,128)(2,1)} reshape(bf16[64,16,2,2,2,64]{5,4,3,2,1,0:T(2,128)(2,1)S(1)} %get-tuple-element.6) | data formatting | bytes 2097152 | tf_op jit(solution)/shard_map/jit(_where)/select_n | solution.py:324
  18.1 0.0 copy-done.1
  18.1 0.7 %reshape.72.rate_ref = f32[2,32,128]{2,1,0:T(8,128)} reshape(f32[2,64,64]{2,1,0:T(8,128)S(1)} %copy-done.1) | data formatting | bytes 65536 | tf_op jit(solution)/shard_map/reshape | solution.py:375
  18.8 0.0 copy-done.2
  18.8 0.7 %reshape.73.angle_ref = f32[2,32,128]{2,1,0:T(8,128)} reshape(f32[2,64,64]{2,1,0:T(8,128)S(1)} %copy-done.2) | data formatting | bytes 65536 | tf_op jit(solution)/shard_map/reshape | solution.py:375
  19.5 40.6 %shard_map.136 = bf16[128,2048]{1,0:T(8,128)(2,1)} custom-call(bf16[128,2048]{1,0:T(8,128)(2,1)} %tokens_ref.1, f32[1,128]{1,0:T(1,128)} %bitcast.13, f32[1,2048]{1,0:T(1,128)} %bitcast.9, bf16[1024,512]{1,0:T(8,128)(2,1)} %select_n.30.drive_ref, bf16[1024,512]{1,0:T(8,128)(2,1)} %convert_element_type.12.read_ref, f32[2,32,128]{2,1,0:T(8,128)} %reshape.72.rate_ref, ...), custom_call_target="tpu_custom_call" | custom-call | tf_op jit(solution)/shard_map/pallas_call | solution.py:336
  60.1 1.9 %copy.18 = bf16[128,2048]{1,0:T(8,128)(2,1)} copy(bf16[128,2048]{1,0:T(8,128)(2,1)} %shard_map.136) | data formatting | bytes 1048576
  (1 shorter events, 0.0 us)
Async XLA Ops:
  0.0 3.0 %copy-start = (bf16[2,2,64,64,16]{3,4,2,1,0:T(8,128)(2,1)S(1)}, bf16[2,2,64,64,16]{3,4,2,1,0:T(8,128)(2,1)}, u32[]{:S(2)}) copy-start(bf16[2,2,64,64,16]{3,4,2,1,0:T(8,128)(2,1)} %param.18) | copy-start | bytes 1572868
  16.1 2.0 %copy-start.1 = (f32[2,64,64]{2,1,0:T(8,128)S(1)}, f32[2,64,64]{2,1,0:T(8,128)}, u32[]{:S(2)}) copy-start(f32[2,64,64]{2,1,0:T(8,128)} %param.20) | copy-start | bytes 98308
  16.1 2.7 %copy-start.2 = (f32[2,64,64]{2,1,0:T(8,128)S(1)}, f32[2,64,64]{2,1,0:T(8,128)}, u32[]{:S(2)}) copy-start(f32[2,64,64]{2,1,0:T(8,128)} %param.21) | copy-start | bytes 98308

commit v2 on v1

--- a/solution.py
+++ b/solution.py
@@ -3,6 +3,7 @@
 
 import jax
 import jax.numpy as jnp
+import numpy as np
 from jax import lax
 from jax.experimental import pallas as pl
 from jax.experimental.pallas import tpu as pltpu
@@ -10,6 +11,8 @@
 
 epsilon = 1e-06
 LANES = 128
+NODES = 16
+SPAN = 3.0
 SUB = 8
 SIN = (4.44288292, -7.30824569, 3.60635422, -0.84611165, 0.10982452)
 COS = (1.41421356, -6.97886411, 5.73988154, -1.88827492, 0.33225154, -0.03450161)
@@ -49,10 +52,11 @@
 
 def kernel(
     sp_size, tp_size,
-    tokens_ref, elapsed_ref, norm_ref, drive_ref, read_ref, rate_ref, angle_ref,
-    skip_ref, bias_ref, gain_ref, in_hbm, glu_hbm, out_hbm,
+    tokens_ref, elapsed_ref, norm_ref, rate_raw, angle_raw, skip_ref, bias_ref, gain_ref,
+    basis_ref, node_ref, drive_hbm, in_hbm, read_hbm, glu_hbm, out_hbm,
     mixed_ref,
-    in_ref, glu_ref, out_ref, e_ref, driven_ref, proj_ref, sre, sim, pre, pim,
+    drive_raw, in_ref, read_raw, glu_ref, out_ref, rate_ref, angle_ref, drive_ref, read_ref,
+    rhs_ref, dec_ref, driven_ref, proj_ref, sre, sim, pre, pim,
     ends, segs, st_ref, resp_ref,
     send1, recv1, send2, recv2, send3, recv3,
     wsem, s1s, r1s, s2s, r2s, s3s, r3s,
@@ -60,6 +64,9 @@
     rows = tokens_ref.shape[0]
     steps = rows // SUB
     pairs = rate_ref.shape[1]
+    states = rate_raw.shape[2]
+    share = LANES // states
+    group_width = driven_ref.shape[1] // rate_raw.shape[1]
     per = pairs // tp_size
     blocks = driven_ref.shape[1] // LANES
     inner = pairs // blocks
@@ -68,7 +75,10 @@
 
     loads = [
         pltpu.make_async_copy(a, b, wsem.at[i])
-        for i, (a, b) in enumerate(((in_hbm, in_ref), (glu_hbm, glu_ref), (out_hbm, out_ref)))
+        for i, (a, b) in enumerate((
+            (drive_hbm, drive_raw), (in_hbm, in_ref), (read_hbm, read_raw),
+            (glu_hbm, glu_ref), (out_hbm, out_ref),
+        ))
     ]
     for load in loads:
         load.start()
@@ -91,34 +101,84 @@
     back = (at_row == (at_col & (SUB - 1)) * steps + (at_col >> 3)).astype(F32).astype(BF16)
     e_row = elapsed_ref[...]
     total_time = jnp.sum(e_row, axis=1, keepdims=True)
-    e_ref[...] = jnp.broadcast_to(
+    e_col = jnp.broadcast_to(
         jnp.sum(jnp.where(place, e_row, 0.0), axis=1, keepdims=True), (rows, LANES)
     )
+    x = e_col * (2.0 / SPAN) - 1.0
+    older, newer = jnp.ones_like(x), x
+    lagrange = basis_ref[0:1, :] + basis_ref[1:2, :] * x
+    for n in range(2, NODES):
+        older, newer = newer, 2.0 * x * newer - older
+        lagrange = lagrange + basis_ref[n : n + 1, :] * newer
+    part = lax.broadcasted_iota(jnp.int32, (rows, LANES), 1) // NODES
+
+    def split(values):
+        high = values.astype(BF16).astype(F32)
+        rest = values - high
+        middle = rest.astype(BF16).astype(F32)
+        return high, middle, rest - middle
+
+    def factor(values):
+        high, middle, low = split(values)
+        picked = jnp.where(part < 3, high, jnp.where(part < 5, middle, low))
+        return jnp.where(part < 6, picked, 0.0).astype(BF16)
+
+    basis = factor(lagrange)
+    rooted = factor(lagrange * jnp.sqrt(e_col))
+    for k in range(2):
+        for raw, packed in ((rate_raw, rate_ref), (angle_raw, angle_ref)):
+            packed[k] = jnp.concatenate(
+                [raw[k, pl.ds(m, pairs, stride=share), :] for m in range(share)], axis=1
+            )
+    owner = lax.broadcasted_iota(jnp.int32, (LANES, states), 0) // group_width % share
+
+    def spread(raw, target, start, at_row, negate):
+        for k in range(2):
+            for c in range(2):
+                piece = raw[k, c, pl.ds(start, LANES), :].astype(F32)
+                if negate and c == 1:
+                    piece = -piece
+                target[pl.ds(at_row, LANES), (2 * k + c) * LANES : (2 * k + c + 1) * LANES] = (
+                    jnp.concatenate(
+                        [jnp.where(owner == m, piece, 0.0) for m in range(share)], axis=1
+                    ).astype(BF16)
+                )
 
     values = tokens_ref[...].astype(F32)
     scale = lax.rsqrt(jnp.mean(values * values, axis=-1, keepdims=True) + epsilon)
     normed = (values * scale * norm_ref[...]).astype(BF16)
-    loads[0].wait()
+    loads[1].wait()
     driven = jnp.dot(normed, in_ref[...], preferred_element_type=F32).astype(BF16)
     driven_ref[...] = jnp.dot(permute, driven, preferred_element_type=F32).astype(BF16)
 
     lane = lax.broadcasted_iota(jnp.int32, (1, LANES), 1)
 
+    nodes = node_ref[...]
+
+    def tabulate(k, r):
+        rate = rate_ref[k, pl.ds(r, 1), :]
+        angle = angle_ref[k, pl.ds(r, 1), :]
+        y = nodes * (rate * 2.0)
+        fade = jnp.exp2(nodes * (rate * (-math.log2(math.e))))
+        rise = one_less_exp(y, fade) / nodes
+        root = rise * lax.rsqrt(jnp.maximum(rise, 1e-36))
+        cosine, sine = cos_sin(nodes * (angle * (0.5 / math.pi)))
+        for at, values in ((2 * k, fade * cosine), (2 * k + 1, fade * sine), (4 + k, root)):
+            parts = split(values)
+            for n, which in enumerate((0, 1, 2, 0, 1, 0, 0, 0)):
+                rhs_ref[n * NODES : (n + 1) * NODES, at * LANES : (at + 1) * LANES] = (
+                    parts[which].astype(BF16)
+                )
+
     def unit(k, r):
-        rate = rate_ref[k, pl.ds(r, 1), :]
-        twice = jnp.broadcast_to(rate * 2.0, (SUB, LANES))
-        slope = jnp.broadcast_to(rate * (-math.log2(math.e)), (SUB, LANES))
-        spin = jnp.broadcast_to(angle_ref[k, pl.ds(r, 1), :] * (0.5 / math.pi), (SUB, LANES))
         state = prod = None
         order = range(steps) if k == 0 else range(steps - 1, -1, -1)
         for j in order:
             at = slice(j * SUB, (j + 1) * SUB)
-            e = e_ref[at, :]
-            fade = jnp.exp2(e * slope)
-            rise = one_less_exp(e * twice, fade)
-            damping = rise * lax.rsqrt(jnp.maximum(rise, 1e-36))
-            cosine, sine = cos_sin(e * spin)
-            decay = (fade * cosine, fade * sine)
+            decay = (
+                dec_ref[at, k * 256 : k * 256 + 128], dec_ref[at, k * 256 + 128 : k * 256 + 256]
+            )
+            damping = dec_ref[at, 512 + k * 128 : 640 + k * 128]
             push_re = proj_ref[at, k * 256 : k * 256 + 128] * damping
             push_im = proj_ref[at, k * 256 + 128 : k * 256 + 256] * damping
             if state is None:
@@ -139,17 +199,23 @@
     def block(b, carry):
         start = pl.multiple_of(b * LANES, LANES)
         piece = driven_ref[:, pl.ds(start, LANES)]
-        weight = drive_ref[pl.ds(start, LANES), :]
+        spread(drive_raw, drive_ref, start, 0, False)
+        weight = drive_ref[...]
 
         def one(i, carry):
             mask = (lane // wide == i).astype(F32).astype(BF16)
             proj_ref[...] = jnp.dot(piece * mask, weight, preferred_element_type=F32)
+            tabulate(0, b * inner + i)
+            tabulate(1, b * inner + i)
+            dec_ref[:, :512] = jnp.dot(basis, rhs_ref[:, :512], preferred_element_type=F32)
+            dec_ref[:, 512:] = jnp.dot(rooted, rhs_ref[:, 512:], preferred_element_type=F32)
             unit(0, b * inner + i)
             unit(1, b * inner + i)
             return carry
 
         return lax.fori_loop(0, inner, one, carry)
 
+    loads[0].wait()
     lax.fori_loop(0, blocks, block, 0)
 
     sub = lax.broadcasted_iota(jnp.int32, (per, SUB, LANES), 1)
@@ -181,7 +247,7 @@
 
     pl.semaphore_wait(barrier, tp_size + sp_size - 2)
 
-    def exchange_tp(send, recv, ssem, rsem):
+    def exchange_tp(send, recv, ssem, rsem, meanwhile=None):
         outs = []
         for off in range(1, tp_size):
             peer = lax.rem(my_tp + off, tp_size)
@@ -193,6 +259,8 @@
             copy.start()
             outs.append(copy)
         recv[my_tp] = send[my_tp]
+        if meanwhile is not None:
+            meanwhile()
         for off in range(1, tp_size):
             peer = lax.rem(my_tp + off, tp_size)
             pltpu.make_async_remote_copy(
@@ -202,7 +270,17 @@
             ).wait_recv()
         return outs
 
-    pending = exchange_tp(send1, recv1, s1s, r1s)
+    def prepare_read():
+        loads[2].wait()
+
+        def piece(b, carry):
+            start = pl.multiple_of(b * LANES, LANES)
+            spread(read_raw, read_ref, start, start, True)
+            return carry
+
+        lax.fori_loop(0, blocks, piece, 0)
+
+    pending = exchange_tp(send1, recv1, s1s, r1s, prepare_read)
     mine = pl.ds(my_tp * per, per)
     rate = (rate_ref[0, mine, :], rate_ref[1, mine, :])
     angle = (angle_ref[0, mine, :], angle_ref[1, mine, :])
@@ -295,11 +373,11 @@
 
     response = resp_ref[...] + skip_ref[...] * driven_ref[...].astype(F32)
     active = jax.nn.gelu(response)
-    loads[1].wait()
+    loads[3].wait()
     gate = jnp.dot(active.astype(BF16), glu_ref[...], preferred_element_type=F32) + bias_ref[...]
     gated = (active * jax.nn.sigmoid(gate)).astype(BF16)
     gated = jnp.dot(back, gated, preferred_element_type=F32).astype(BF16)
-    loads[2].wait()
+    loads[4].wait()
     projected = jnp.dot(gated, out_ref[...], preferred_element_type=F32)
     scale = lax.rsqrt(jnp.mean(projected * projected, axis=-1, keepdims=True) + epsilon)
     mixed_ref[...] = (projected * scale * gain_ref[...]).astype(BF16)
@@ -317,17 +395,12 @@
     share = LANES // states
     pairs = groups // share
     per = pairs // tp_size
-    parity = (jnp.arange(groups)[:, None] % share == jnp.arange(share)[None, :])
-    parity = parity[:, None, None, None, :, None]
-
-    def spread(values):
-        return jnp.where(parity, values[:, :, :, :, None, :], 0).astype(BF16).reshape(
-            channels, 4 * LANES
-        )
-
-    drive = spread(state_input.transpose(2, 4, 0, 1, 3))
-    sign = jnp.array([1.0, -1.0], F32)[None, :, None, None, None]
-    read = spread((state_output * sign).transpose(2, 3, 0, 1, 4))
+    drive = state_input.transpose(0, 1, 2, 4, 3).reshape(2, 2, channels, states)
+    read = state_output.reshape(2, 2, channels, states)
+    turns = np.pi * (np.arange(LANES) % NODES + 0.5) / NODES
+    orders = np.arange(NODES)[:, None]
+    basis = np.cos(orders * turns[None, :]) * np.where(orders == 0, 1, 2) / NODES
+    nodes = np.broadcast_to((np.cos(turns[:NODES, None]) + 1) * (SPAN / 2), (NODES, LANES))
 
     vmem = pl.BlockSpec(memory_space=pltpu.VMEM)
     hbm = pl.BlockSpec(memory_space=pl.ANY)
@@ -336,13 +409,20 @@
     return pl.pallas_call(
         functools.partial(kernel, sp_size, tp_size),
         out_shape=jax.ShapeDtypeStruct((rows, width), BF16),
-        in_specs=[vmem] * 10 + [hbm] * 3,
+        in_specs=[vmem] * 10 + [hbm] * 5,
         out_specs=vmem,
         scratch_shapes=[
+            pltpu.VMEM(drive.shape, BF16),
             pltpu.VMEM(in_weight.shape, BF16),
+            pltpu.VMEM(read.shape, F32),
             pltpu.VMEM(glu_weight.shape, BF16),
             pltpu.VMEM(out_weight.shape, BF16),
-            pltpu.VMEM((rows, LANES), F32),
+            pltpu.VMEM((2, pairs, LANES), F32),
+            pltpu.VMEM((2, pairs, LANES), F32),
+            pltpu.VMEM((LANES, 4 * LANES), BF16),
+            pltpu.VMEM((channels, 4 * LANES), BF16),
+            pltpu.VMEM((LANES, 6 * LANES), BF16),
+            pltpu.VMEM((rows, 6 * LANES), F32),
             pltpu.VMEM((rows, channels), BF16),
             pltpu.VMEM((rows, 4 * LANES), F32),
             pltpu.VMEM(cells, F32),
@@ -359,7 +439,7 @@
             pltpu.VMEM((sp_size, 5, per, LANES), F32),
             pltpu.VMEM((tp_size, 4, per, LANES), F32),
             pltpu.VMEM((tp_size, 4, per, LANES), F32),
-            dma((3,)),
+            dma((5,)),
             dma((tp_size,)),
             dma((tp_size,)),
             dma((sp_size,)),
@@ -371,10 +451,10 @@
             collective_id=0, has_side_effects=True, vmem_limit_bytes=60 * 1024 * 1024
         ),
     )(
-        tokens, elapsed.reshape(1, rows), norm_gain.reshape(1, -1), drive, read,
-        forget_rate.reshape(2, pairs, LANES), decay_angle.reshape(2, pairs, LANES),
+        tokens, elapsed.reshape(1, rows), norm_gain.reshape(1, -1), forget_rate, decay_angle,
         skip_gain.reshape(1, -1), glu_bias.reshape(1, -1), out_gain.reshape(1, -1),
-        in_weight, glu_weight, out_weight,
+        jnp.asarray(basis, F32), jnp.asarray(nodes, F32),
+        drive, in_weight, read, glu_weight, out_weight,
     )
 
 

time: 62.2 us -> 42.2 us (0.68)
  local copies, waits for them, and re-layouts: 13.4 us -> 1.88 us
  other arithmetic: 7.92 us -> 0 us
    convert_element_type x1 -> x0, local copies, waits for them, and re-layouts: 5.98 us -> none  [spread(): jnp.where(parity, values[:, :, :, :, None, :], 0).astype(BF16)]
    convert_element_type x1 -> x0, other arithmetic: 5.92 us -> none  [spread(): jnp.where(parity, values[:, :, :, :, None, :], 0).astype(BF16)]
    transpose x2 -> x0, local copies, waits for them, and re-layouts: 2.16 us -> none  [the longest x1 1.08 us: local(): read = spread((state_output * sign).transpose(2, 3, 0, 1, 4))]
    select_n x1 -> x0, local copies, waits for them, and re-layouts: 2.02 us -> none  [spread(): jnp.where(parity, values[:, :, :, :, None, :], 0).astype(BF16)]
    transpose x1 -> x0, other arithmetic: 1.92 us -> none  [local(): read = spread((state_output * sign).transpose(2, 3, 0, 1, 4))]
    reshape x2 -> x0, local copies, waits for them, and re-layouts: 1.37 us -> none  [the longest x1 0.69 us: local(): forget_rate.reshape(2, pairs, LANES)]
    unnamed x7 -> x1, local copies, waits for them, and re-layouts: 1.89 us -> 1.88 us
where the time goes in v2:
time: 42.2 us; the launch traced here: 42.1 us
  Pallas kernels  40.2 us (95%)
  local copies, waits for them, and re-layouts  1.88 us (4%)
    pallas_call x1, Pallas kernels, local(): pl.pallas_call(functools.partial(kernel, sp_size, tp_size), out_shape=jax...  40.2 us
    unnamed x1, local copies, waits for them, and re-layouts  1.88 us

profile of v2, /device:TPU:0, one launch (start us, length us, event | category | flops | bytes accessed | tf_op | source)
XLA Modules:
  0.0 42.1 jit_solution(15187026325620446013)
XLA Ops:
  0.0 40.2 %shard_map.145 = bf16[128,2048]{1,0:T(8,128)(2,1)} custom-call(bf16[128,2048]{1,0:T(8,128)(2,1)} %tokens_ref.1, f32[1,128]{1,0:T(1,128)} %bitcast.15, f32[1,2048]{1,0:T(1,128)} %bitcast.11, f32[2,64,64]{2,1,0:T(8,128)} %rate_raw.1, f32[2,64,64]{2,1,0:T(8,128)} %angle_raw.1, f32[1,1024]{1,0:T(1,128)} %bitcast.13, f32[1,1024]{1,0:T(1,128)} %bitcast.14, ...), custom_call_target="tpu_custom_call" | custom-call | tf_op jit(solution)/shard_map/pallas_call | solution.py:409
  40.2 1.9 %copy.17 = bf16[128,2048]{1,0:T(8,128)(2,1)} copy(bf16[128,2048]{1,0:T(8,128)(2,1)} %shard_map.145) | data formatting | bytes 1048576

commit v3 on v2

--- a/solution.py
+++ b/solution.py
@@ -80,7 +80,7 @@
             (glu_hbm, glu_ref), (out_hbm, out_ref),
         ))
     ]
-    for load in loads:
+    for load in loads[:2]:
         load.start()
     barrier = pltpu.get_barrier_semaphore()
     for off in range(1, tp_size):
@@ -144,15 +144,6 @@
                     ).astype(BF16)
                 )
 
-    values = tokens_ref[...].astype(F32)
-    scale = lax.rsqrt(jnp.mean(values * values, axis=-1, keepdims=True) + epsilon)
-    normed = (values * scale * norm_ref[...]).astype(BF16)
-    loads[1].wait()
-    driven = jnp.dot(normed, in_ref[...], preferred_element_type=F32).astype(BF16)
-    driven_ref[...] = jnp.dot(permute, driven, preferred_element_type=F32).astype(BF16)
-
-    lane = lax.broadcasted_iota(jnp.int32, (1, LANES), 1)
-
     nodes = node_ref[...]
 
     def tabulate(k, r):
@@ -166,11 +157,29 @@
         for at, values in ((2 * k, fade * cosine), (2 * k + 1, fade * sine), (4 + k, root)):
             parts = split(values)
             for n, which in enumerate((0, 1, 2, 0, 1, 0, 0, 0)):
-                rhs_ref[n * NODES : (n + 1) * NODES, at * LANES : (at + 1) * LANES] = (
+                rhs_ref[r, n * NODES : (n + 1) * NODES, at * LANES : (at + 1) * LANES] = (
                     parts[which].astype(BF16)
                 )
 
-    def unit(k, r):
+    def tabulate_pair(r, carry):
+        tabulate(0, r)
+        tabulate(1, r)
+        return carry
+
+    lax.fori_loop(0, pairs, tabulate_pair, 0)
+
+    values = tokens_ref[...].astype(F32)
+    scale = lax.rsqrt(jnp.mean(values * values, axis=-1, keepdims=True) + epsilon)
+    normed = (values * scale * norm_ref[...]).astype(BF16)
+    loads[1].wait()
+    for load in loads[2:]:
+        load.start()
+    driven = jnp.dot(normed, in_ref[...], preferred_element_type=F32).astype(BF16)
+    driven_ref[...] = jnp.dot(permute, driven, preferred_element_type=F32).astype(BF16)
+
+    lane = lax.broadcasted_iota(jnp.int32, (1, LANES), 1)
+
+    def unit(k, r, dec_ref, proj_ref):
         state = prod = None
         order = range(steps) if k == 0 else range(steps - 1, -1, -1)
         for j in order:
@@ -202,18 +211,19 @@
         spread(drive_raw, drive_ref, start, 0, False)
         weight = drive_ref[...]
 
-        def one(i, carry):
+        for i in range(inner):
+            r = b * inner + i
             mask = (lane // wide == i).astype(F32).astype(BF16)
-            proj_ref[...] = jnp.dot(piece * mask, weight, preferred_element_type=F32)
-            tabulate(0, b * inner + i)
-            tabulate(1, b * inner + i)
-            dec_ref[:, :512] = jnp.dot(basis, rhs_ref[:, :512], preferred_element_type=F32)
-            dec_ref[:, 512:] = jnp.dot(rooted, rhs_ref[:, 512:], preferred_element_type=F32)
-            unit(0, b * inner + i)
-            unit(1, b * inner + i)
-            return carry
-
-        return lax.fori_loop(0, inner, one, carry)
+            proj_ref[i] = jnp.dot(piece * mask, weight, preferred_element_type=F32)
+            dec_ref[i, :, :512] = jnp.dot(
+                basis, rhs_ref[r, :, :512], preferred_element_type=F32
+            )
+            dec_ref[i, :, 512:] = jnp.dot(
+                rooted, rhs_ref[r, :, 512:], preferred_element_type=F32
+            )
+            unit(0, r, dec_ref.at[i], proj_ref.at[i])
+            unit(1, r, dec_ref.at[i], proj_ref.at[i])
+        return carry
 
     loads[0].wait()
     lax.fori_loop(0, blocks, block, 0)
@@ -342,7 +352,7 @@
         start = pl.multiple_of(b * LANES, LANES)
         weight = read_ref[pl.ds(start, LANES), :]
 
-        def one(i, total):
+        def one(i):
             r = b * inner + i
             q, row = r // per, lax.rem(r, per)
             for k in range(2):
@@ -357,16 +367,17 @@
                 moved = cmul(prod, enter)
                 whole_re = sre[k, r].reshape(shape) + moved[0]
                 whole_im = sim[k, r].reshape(shape) + moved[1]
-                st_ref[:, k * 256 : k * 256 + 128] = whole_re.reshape(rows, LANES).astype(BF16)
-                st_ref[:, k * 256 + 128 : k * 256 + 256] = whole_im.reshape(rows, LANES).astype(BF16)
+                st_ref[i, :, k * 256 : k * 256 + 128] = whole_re.reshape(rows, LANES).astype(BF16)
+                st_ref[i, :, k * 256 + 128 : k * 256 + 256] = whole_im.reshape(rows, LANES).astype(BF16)
             out = lax.dot_general(
-                st_ref[...], weight, (((1,), (1,)), ((), ())), preferred_element_type=F32
-            )
-            return jnp.where(lane // wide == i, out, total)
-
-        resp_ref[:, pl.ds(start, LANES)] = lax.fori_loop(
-            0, inner, one, jnp.zeros((rows, LANES), F32)
-        )
+                st_ref[i], weight, (((1,), (1,)), ((), ())), preferred_element_type=F32
+            )
+            return jnp.where(lane // wide == i, out, 0.0)
+
+        total = one(0)
+        for i in range(1, inner):
+            total = total + one(i)
+        resp_ref[:, pl.ds(start, LANES)] = total
         return carry
 
     lax.fori_loop(0, blocks, read_block, 0)
@@ -395,6 +406,7 @@
     share = LANES // states
     pairs = groups // share
     per = pairs // tp_size
+    inner = pairs // (channels // LANES)
     drive = state_input.transpose(0, 1, 2, 4, 3).reshape(2, 2, channels, states)
     read = state_output.reshape(2, 2, channels, states)
     turns = np.pi * (np.arange(LANES) % NODES + 0.5) / NODES
@@ -421,17 +433,17 @@
             pltpu.VMEM((2, pairs, LANES), F32),
             pltpu.VMEM((LANES, 4 * LANES), BF16),
             pltpu.VMEM((channels, 4 * LANES), BF16),
-            pltpu.VMEM((LANES, 6 * LANES), BF16),
-            pltpu.VMEM((rows, 6 * LANES), F32),
+            pltpu.VMEM((pairs, LANES, 6 * LANES), BF16),
+            pltpu.VMEM((inner, rows, 6 * LANES), F32),
             pltpu.VMEM((rows, channels), BF16),
-            pltpu.VMEM((rows, 4 * LANES), F32),
+            pltpu.VMEM((inner, rows, 4 * LANES), F32),
             pltpu.VMEM(cells, F32),
             pltpu.VMEM(cells, F32),
             pltpu.VMEM(cells, F32),
             pltpu.VMEM(cells, F32),
             pltpu.VMEM((2, 4, pairs, SUB, LANES), F32),
             pltpu.VMEM((2, 4, pairs, SUB, LANES), F32),
-            pltpu.VMEM((rows, 4 * LANES), BF16),
+            pltpu.VMEM((inner, rows, 4 * LANES), BF16),
             pltpu.VMEM((rows, channels), F32),
             pltpu.VMEM((tp_size, 5, per, LANES), F32),
             pltpu.VMEM((tp_size, 5, per, LANES), F32),

time: 42.2 us -> 32.9 us (0.78)
  Pallas kernels: 40.2 us -> 30.9 us
    pallas_call x1, Pallas kernels: 40.2 us -> 30.9 us  [local(): pl.pallas_call(functools.partial(kernel, sp_size, tp_size), out_shape=jax...]
where the time goes in v3:
time: 32.9 us; the launch traced here: 32.8 us
  Pallas kernels  30.9 us (94%)
  local copies, waits for them, and re-layouts  1.88 us (6%)
    pallas_call x1, Pallas kernels, local(): pl.pallas_call(functools.partial(kernel, sp_size, tp_size), out_shape=jax...  30.9 us
    unnamed x1, local copies, waits for them, and re-layouts  1.88 us

profile of v3, /device:TPU:0, one launch (start us, length us, event | category | flops | bytes accessed | tf_op | source)
XLA Modules:
  0.0 32.8 jit_solution(1845359133381350813)
XLA Ops:
  0.0 30.9 %shard_map.145 = bf16[128,2048]{1,0:T(8,128)(2,1)} custom-call(bf16[128,2048]{1,0:T(8,128)(2,1)} %tokens_ref.1, f32[1,128]{1,0:T(1,128)} %bitcast.15, f32[1,2048]{1,0:T(1,128)} %bitcast.11, f32[2,64,64]{2,1,0:T(8,128)} %rate_raw.1, f32[2,64,64]{2,1,0:T(8,128)} %angle_raw.1, f32[1,1024]{1,0:T(1,128)} %bitcast.13, f32[1,1024]{1,0:T(1,128)} %bitcast.14, ...), custom_call_target="tpu_custom_call" | custom-call | tf_op jit(solution)/shard_map/pallas_call | solution.py:421
  30.9 1.9 %copy.17 = bf16[128,2048]{1,0:T(8,128)(2,1)} copy(bf16[128,2048]{1,0:T(8,128)(2,1)} %shard_map.145) | data formatting | bytes 1048576
